TPU v7x, 512 devices: a whole 4x4x16 slice. The times are simulated.
512 devices in a mesh: sp: 32 (over z, core), tp: 16 (over y, x).
Axes of the slice: x: 4, y: 4, z: 16, core: 2. Of those that a mesh axis runs over, the one named last changes fastest.
Arguments:
- residual: bfloat16 [4096, 2048], P('sp'), may hold values from -45 to 45
- query_a: bfloat16 [4096, 16, 128], P('sp', 'tp'), may hold values from -125 to 125
- keys_a: bfloat16 [4096, 16, 128], P('sp', 'tp'), may hold values from -8 to 8
- values_a: bfloat16 [4096, 16, 128], P('sp', 'tp'), may hold values from -6 to 6
- query_b: bfloat16 [4096, 16, 256], P('sp', 'tp'), may hold values from -125 to 125
- keys_b: bfloat16 [4096, 16, 256], P('sp', 'tp'), may hold values from -8 to 8
- values_b: bfloat16 [4096, 16, 256], P('sp', 'tp'), may hold values from -6 to 6
- lambda_a: float32 [16], P('tp'), may hold values from 0.3 to 0.8
- lambda_b: float32 [16], P('tp'), may hold values from 0.3 to 0.8
- gain_a: float32 [128], replicated, may hold values from 0.1 to 1.9
- gain_b: float32 [256], replicated, may hold values from 0.1 to 1.9
- proj_a: bfloat16 [2048, 2048], P('tp'), may hold values from -0.078125 to 0.078125
- proj_b: bfloat16 [4096, 2048], P('tp'), may hold values from -0.078125 to 0.078125
- norm_gain: float32 [2048], replicated, may hold values from 0.1 to 1.9
- routes: int32 [4096, 2], P('sp'), may hold values from 0 to 31, all different within a row; in each aligned block of 128 rows (0 to 127, 128 to 255, ...) at most 16 rows name the same one
- route_weight: float32 [4096, 2], P('sp'), may hold values from 0.2 to 2
- expert_gate: bfloat16 [32, 2048, 2048], P('sp', None, 'tp'), may hold values from -0.125 to 0.125
- expert_up: bfloat16 [32, 2048, 2048], P('sp', None, 'tp'), may hold values from -0.125 to 0.125
- expert_down: bfloat16 [32, 2048, 2048], P('sp', 'tp'), may hold values from -0.125 to 0.125
Outputs:
- layer_out: bfloat16 [4096, 2048], P('sp', 'tp')
Inputs may be any that keep to these rules, and one draw needn't show every extreme that they name: `routes`: each row names 2 different experts; in each aligned block of 128 rows no expert is named more than 16 times, a bound that some block reaches.
All inputs are finite; a program needn't handle non-finite values.
Results may differ from a plain program's by a relative error of at most 0.013.
Values may be sent and summed in bfloat16 or wider, within the bound.
No kernel may reach another device: no remote copies, remote signals or barrier semaphores. Data moves between devices by JAX's collectives and lax.ppermute only.
A program may use at most 64 MiB of HBM per device.

v0:
```python
import jax
import jax.numpy as jnp
from jax import lax
from jax.sharding import PartitionSpec as P

DK_A = 64
DK_B = 128
SEG = 64
TOP = 2


EPS = 1e-06


def side_by_side(arrays, axis, dim, along):
    ends, at = ([], 0)
    for a in arrays[:-1]:
        at += a.shape[along]
        ends.append(at)
    both = jnp.concatenate(arrays, axis=along)
    return tuple(jnp.split(lax.all_gather(both, axis, axis=dim, tiled=True), ends, axis=along))


def split_up(value, dim, count):
    dims = value.shape
    pieces = value.reshape(*dims[:dim], count, dims[dim] // count, *dims[dim + 1 :])
    return jnp.moveaxis(pieces, dim, 0)


def summed_on_arrival(value, axis, dim):
    pieces = split_up(value, dim, lax.axis_size(axis))
    arrived = lax.all_to_all(pieces, axis, split_axis=0, concat_axis=0, tiled=True)
    return arrived.astype(jnp.float32).sum(axis=0)


def sent_to_all(value, axis):
    copies = jnp.broadcast_to(value, (lax.axis_size(axis), *value.shape))
    return lax.all_to_all(copies, axis, split_axis=0, concat_axis=0, tiled=True)


def over_copies(value, axis):
    everything = sent_to_all(value, axis)
    return jnp.sum(everything, axis=0)


def in_order(pieces, dim):
    pieces = jnp.moveaxis(pieces, 0, dim)
    dims = pieces.shape
    return pieces.reshape(*dims[:dim], dims[dim] * dims[dim + 1], *dims[dim + 2 :])


def gather_directly(value, axis, dim):
    return in_order(sent_to_all(value, axis), dim)


def attend_local(queries, keys_all, values_all, mixing, head_gain, key_size, offset, block_rows):
    tok_rows = queries.shape[0]
    heads_local = queries.shape[1]
    positions = offset + jnp.arange(tok_rows, dtype=jnp.int32)
    query_seg = positions // SEG
    factor = key_size ** (-0.5)
    needed = (offset + tok_rows + block_rows - 1) // block_rows
    first_query = queries[..., :key_size]
    second_query = queries[..., key_size:]

    def block_scores(start, map_query, block_keys):
        raw_scores = (
            jnp.einsum("qhd,khd->hqk", map_query, block_keys, preferred_element_type=jnp.float32)
            * factor
        )
        key_seg = (start + jnp.arange(block_rows, dtype=jnp.int32)) // SEG
        visible = query_seg[:, None] >= key_seg[None, :]
        return jnp.where(visible[None], raw_scores, -jnp.inf)

    def both_scores(block_index):
        start = block_index * block_rows
        block_keys = lax.dynamic_slice_in_dim(keys_all, start, block_rows, 0)
        first_scores = block_scores(start, first_query, block_keys[..., :key_size])
        second_scores = block_scores(start, second_query, block_keys[..., key_size:])
        return (start, first_scores, second_scores)

    def update(old_max, old_sum, scores):
        new_max = jnp.maximum(old_max, jnp.max(scores, axis=-1, keepdims=True))
        new_sum = old_sum * jnp.exp(old_max - new_max) + jnp.sum(
            jnp.exp(scores - new_max), axis=-1, keepdims=True
        )
        return (new_max, new_sum)

    def statistics(block_index, running):
        first_max, first_sum, second_max, second_sum = running
        start, first_scores, second_scores = both_scores(block_index)
        first_max, first_sum = update(first_max, first_sum, first_scores)
        second_max, second_sum = update(second_max, second_sum, second_scores)
        return (first_max, first_sum, second_max, second_sum)

    start_max = jnp.full((heads_local, tok_rows, 1), -jnp.inf, jnp.float32)
    start_sum = jnp.zeros((heads_local, tok_rows, 1), jnp.float32)
    first_max, first_sum, second_max, second_sum = lax.fori_loop(
        0, needed, statistics, (start_max, start_sum, start_max, start_sum)
    )
    mix_col = mixing[:, None, None]

    def accumulate(block_index, summed_rows):
        start, first_scores, second_scores = both_scores(block_index)
        first_probs = jnp.exp(first_scores - first_max) / first_sum
        second_probs = jnp.exp(second_scores - second_max) / second_sum
        block_weights = (first_probs - mix_col * second_probs).astype(jnp.bfloat16)
        block_values = lax.dynamic_slice_in_dim(values_all, start, block_rows, 0)
        return summed_rows + jnp.einsum(
            "hqk,khe->qhe", block_weights, block_values, preferred_element_type=jnp.float32
        )

    mixed = lax.fori_loop(
        0, needed, accumulate, jnp.zeros((tok_rows, heads_local, values_all.shape[2]), jnp.float32)
    )
    mean_sq = jnp.mean(mixed * mixed, axis=-1, keepdims=True)
    return (mixed * lax.rsqrt(mean_sq + EPS) * head_gain).astype(jnp.bfloat16)


def local(
    residual,
    query_a,
    keys_a,
    values_a,
    query_b,
    keys_b,
    values_b,
    lambda_a,
    lambda_b,
    gain_a,
    gain_b,
    proj_a,
    proj_b,
    norm_gain,
    routes,
    route_weight,
    expert_gate,
    expert_up,
    expert_down,
):
    tok_rows = residual.shape[0]
    model_width = residual.shape[1]
    seq_devices = lax.axis_size("sp")
    head_devices = lax.axis_size("tp")
    head_index = lax.axis_index("tp")
    offset = lax.axis_index("sp") * tok_rows
    every_keys_a, every_values_a, every_keys_b, every_values_b = side_by_side(
        (keys_a, values_a, keys_b, values_b), "sp", 0, 2
    )
    block_rows = 512
    heads_a = attend_local(
        query_a, every_keys_a, every_values_a, lambda_a, gain_a, DK_A, offset, block_rows
    )
    heads_b = attend_local(
        query_b, every_keys_b, every_values_b, lambda_b, gain_b, DK_B, offset, block_rows
    )
    partial_branch = jnp.dot(
        heads_a.reshape(tok_rows, -1), proj_a, preferred_element_type=jnp.float32
    )
    partial_branch = partial_branch + jnp.dot(
        heads_b.reshape(tok_rows, -1), proj_b, preferred_element_type=jnp.float32
    )
    columns = model_width // head_devices
    col_start = head_index * columns
    summed_cols = summed_on_arrival(partial_branch.astype(jnp.bfloat16), "tp", 1)
    residual_cols = lax.dynamic_slice_in_dim(residual, col_start, columns, 1)
    stream_cols = (
        (residual_cols.astype(jnp.float32) + summed_cols).astype(jnp.bfloat16).astype(jnp.float32)
    )
    squares = over_copies(jnp.sum(stream_cols * stream_cols, axis=1), "tp")
    row_scale = lax.rsqrt(squares / model_width + EPS)
    gain_cols = lax.dynamic_slice_in_dim(norm_gain, col_start, columns, 0)
    normed_cols = (stream_cols * row_scale[:, None] * gain_cols).astype(jnp.bfloat16)
    slot_count = 2 * tok_rows * TOP // seq_devices
    assign = routes.reshape(-1)
    onehot = (assign[:, None] == jnp.arange(seq_devices, dtype=jnp.int32)[None, :]).astype(
        jnp.int32
    )
    earlier = jnp.cumsum(onehot, axis=0) - onehot
    slot_index = jnp.sum(earlier * onehot, axis=1)
    target = assign * slot_count + slot_index
    placed = (
        target[:, None] == jnp.arange(seq_devices * slot_count, dtype=jnp.int32)[None, :]
    ).reshape(tok_rows, TOP, -1)
    select = jnp.sum(placed.astype(jnp.bfloat16), axis=1)
    gates = route_weight / jnp.sum(route_weight, axis=1, keepdims=True)
    combine = jnp.sum(placed.astype(jnp.float32) * gates[:, :, None], axis=1)
    send_rows = jnp.einsum(
        "ts,td->sd", select, normed_cols, preferred_element_type=jnp.float32
    ).astype(jnp.bfloat16)
    send_rows = send_rows.reshape(seq_devices, slot_count, columns)
    routed_rows = gather_directly(
        lax.all_to_all(send_rows, "sp", split_axis=0, concat_axis=0, tiled=True), "tp", 2
    )
    sources = routed_rows.shape[0]
    count = routed_rows.shape[1]
    flat_rows = routed_rows.reshape(-1, model_width)
    gate_val = jnp.dot(flat_rows, expert_gate[0], preferred_element_type=jnp.float32)
    up_val = jnp.dot(flat_rows, expert_up[0], preferred_element_type=jnp.float32)
    hidden = (jax.nn.silu(gate_val) * up_val).astype(jnp.bfloat16)
    down_part = jnp.dot(hidden, expert_down[0], preferred_element_type=jnp.float32).reshape(
        sources, count, model_width
    )
    results = summed_on_arrival(down_part.astype(jnp.bfloat16), "tp", 2).astype(jnp.bfloat16)
    returned = lax.all_to_all(results, "sp", split_axis=0, concat_axis=0, tiled=True)
    returned_flat = returned.reshape(seq_devices * slot_count, columns).astype(jnp.float32)
    experts_sum = jnp.dot(combine, returned_flat, precision=lax.Precision.HIGHEST)
    return (stream_cols + experts_sum).astype(jnp.bfloat16)


def solution(mesh):
    placed = (
        P("sp", None),
        P("sp", "tp", None),
        P("sp", "tp", None),
        P("sp", "tp", None),
        P("sp", "tp", None),
        P("sp", "tp", None),
        P("sp", "tp", None),
        P("tp"),
        P("tp"),
        P(),
        P(),
        P("tp", None),
        P("tp", None),
        P(),
        P("sp", None),
        P("sp", None),
        P("sp", None, "tp"),
        P("sp", None, "tp"),
        P("sp", "tp", None),
    )
    return jax.shard_map(
        local, mesh=mesh, in_specs=placed, out_specs=P("sp", "tp"), check_vma=False
    )
```

profile of v0, /device:TPU:1, one launch (start us, length us, event | category | flops | bytes accessed | tf_op | source)
XLA Modules:
  0.0 307.4 jit_solution(9099317083835386692)
XLA Ops:
  6.5 1.7 pad_maximum_fusion
  8.2 0.0 all-gather.2.cloned.1.call-update
  8.2 0.9 fusion.150
  9.1 0.1 copy.92
  9.2 0.1 copy.93
  9.3 0.8 copy.85
  10.1 0.1 eq.43
  10.3 0.8 fusion.149
  11.1 80.3 %all-gather.2.cloned.1.call-done = bf16[4096,1,768]{2,0,1:T(8,128)(2,1)} async-done(((bf16[128,1,768]{2,0,1:T(8,128)(2,1)}), bf16[4096,1,768]{2,0,1:T(8,128)(2,1)}) %all-gather.2.cloned.1.call-update) | async-done | bytes 6291472 | tf_op jit(solution)/shard_map/all_gather | solution.py:21
  91.4 2.7 fusion.147
  94.1 0.5 copy.83
  94.6 0.9 while.64
  94.7 0.3 fusion.171
  95.0 0.1 exponential_reduce_fusion.9
  95.1 0.3 fusion.172
  95.4 0.1 exponential_reduce_fusion.8
  95.5 2.3 while.65
  95.6 0.9 fusion.176
  96.5 1.3 fusion.177
  97.9 3.9 %fusion.148 = (bf16[4096,1,256]{2,0,1:T(8,128)(2,1)S(1)}, bf16[4096,1,256]{2,0,1:T(8,128)(2,1)}) fusion(bf16[4096,1,768]{2,0,1:T(8,128)(2,1)} %all-gather.2.cloned.1.call-done), kind=kLoop, calls=%fused_computation.228 | loop fusion | bytes 8388608 | tf_op jit(solution)/shard_map/split | solution.py:21
  101.8 0.8 while.66
  101.8 0.2 fusion.178
  102.1 0.1 exponential_reduce_fusion.11
  102.2 0.2 fusion.179
  102.4 0.1 exponential_reduce_fusion.10
  102.6 3.1 %while.67 = (s32[]{:T(128)}, f32[128,1,256]{0,2,1:T(8,128)S(1)}, s32[]{:T(128)}, bf16[4096,1,256]{2,0,1:T(8,128)(2,1)}, bf16[4096,1,256]{2,0,1:T(8,128)(2,1)S(1)...) while((s32[]{:T(128)}, f32[128,1,256]{0,2,1:T(8,128)S(1)}, ...), condition=%wide.region_16.17_spmd.clone, body=%wide.region_15.16_spmd.clone.sunk | while | flops 68003840 | bytes 1388267 | solution.py:113
  102.6 0.9 fusion.183
  103.6 2.1 fusion.184
  105.8 0.4 fusion.128
  106.2 0.5 copy-done.1
  106.8 0.4 fusion.111
  107.2 0.9 copy.114
  108.1 6.5 %all-to-all-start = ((bf16[16,128,128]{2,1,0:T(8,128)(2,1)}), bf16[16,128,128]{2,1,0:T(8,128)(2,1)S(1)}, u32[]{:S(2)}, u32[]{:S(2)}) async-start(bf16[16,128,128]{2,1,0:T(8,128)(2,1)} %bitcast.270), calls=%async_computation | async-start | bytes 1048576 | tf_op jit(solution)/shard_map/all_to_all | solution.py:32
  114.7 0.1 eq.39
  114.8 0.6 reduce-window.6
  115.4 0.2 slice_reduce_fusion
  115.6 0.1 fusion.137
  115.7 0.1 reduce_sum.138
  115.9 0.1 copy.88
  115.9 9.5 %all-to-all-done = bf16[16,128,128]{2,1,0:T(8,128)(2,1)S(1)} async-done(((bf16[16,128,128]{2,1,0:T(8,128)(2,1)}), bf16[16,128,128]{2,1,0:T(8,128)(2,1)S(1)}, u32[]{:S(2)}, u32[]{:S(2)}) %all-to-all-start) | async-done | bytes 524320 | tf_op jit(solution)/shard_map/all_to_all | solution.py:32
  125.5 0.1 convert_reduce_fusion
  125.5 0.9 fusion.124
  126.4 0.6 broadcast_in_dim.122
  127.0 3.5 %all-to-all-start.1 = ((f32[16,1,128]{2,1,0:T(1,128)}), f32[16,1,128]{2,1,0:T(1,128)S(1)}, u32[]{:S(2)}, u32[]{:S(2)}) async-start(f32[16,1,128]{2,1,0:T(1,128)} %broadcast_in_dim.122), calls=%async_computation.1 | async-start | bytes 16384 | tf_op jit(solution)/shard_map/all_to_all | solution.py:38
  130.5 0.1 fusion.123
  130.6 0.8 dynamic_slice.43
  131.4 5.4 %all-to-all-done.1 = f32[16,1,128]{2,1,0:T(1,128)S(1)} async-done(((f32[16,1,128]{2,1,0:T(1,128)}), f32[16,1,128]{2,1,0:T(1,128)S(1)}, u32[]{:S(2)}, u32[]{:S(2)}) %all-to-all-start.1) | async-done | bytes 8224 | tf_op jit(solution)/shard_map/all_to_all | solution.py:38
  136.8 0.3 convolution_convert_fusion.1
  137.1 72.0 %all_to_all.31 = bf16[32,16,128]{2,1,0:T(8,128)(2,1)S(1)} all-to-all(bf16[32,16,128]{2,1,0:T(8,128)(2,1)S(1)} %bitcast.364), channel_id=1, replica_groups=mesh['sp'=32,'tp'=16] {'sp'}, dimensions={0} | all-to-all | bytes 262144 | tf_op jit(solution)/shard_map/all_to_all | solution.py:193
  209.1 0.4 broadcast_in_dim.123
  209.5 29.6 %all_to_all.32 = bf16[16,32,16,128]{3,2,1,0:T(8,128)(2,1)S(1)} all-to-all(bf16[16,32,16,128]{3,2,1,0:T(8,128)(2,1)S(1)} %broadcast_in_dim.123), channel_id=1, replica_groups=mesh['sp'=32,'tp'=16] {'tp'}, dimensions={0} | all-to-all | bytes 4194304 | tf_op jit(solution)/shard_map/all_to_all | solution.py:38
  239.1 2.4 copy.90
  241.6 0.7 fusion.106
  242.3 0.3 copy-done.8
  242.6 0.7 fusion.115
  243.3 0.3 copy-done.2
  243.6 0.7 fusion.110
  244.3 0.5 copy.113
  244.9 28.2 %all_to_all.33 = bf16[16,32,16,128]{3,2,1,0:T(8,128)(2,1)S(1)} all-to-all(bf16[16,32,16,128]{3,2,1,0:T(8,128)(2,1)S(1)} %bitcast.360), channel_id=1, replica_groups=mesh['sp'=32,'tp'=16] {'tp'}, dimensions={0} | all-to-all | bytes 4194304 | tf_op jit(solution)/shard_map/all_to_all | solution.py:32
  273.1 0.9 reduce_sum.144
  274.0 9.8 %all-to-all-start.5 = ((bf16[32,16,128]{2,1,0:T(8,128)(2,1)}), bf16[32,16,128]{2,1,0:T(8,128)(2,1)S(1)}, u32[]{:S(2)}, u32[]{:S(2)}) async-start(bf16[32,16,128]{2,1,0:T(8,128)(2,1)} %reduce_sum.144), calls=%async_computation.5 | async-start | bytes 262144 | tf_op jit(solution)/shard_map/all_to_all | solution.py:205
  283.9 0.1 select_reduce_fusion
  284.1 15.7 %all-to-all-done.5 = bf16[32,16,128]{2,1,0:T(8,128)(2,1)S(1)} async-done(((bf16[32,16,128]{2,1,0:T(8,128)(2,1)}), bf16[32,16,128]{2,1,0:T(8,128)(2,1)S(1)}, u32[]{:S(2)}, u32[]{:S(2)}) %all-to-all-start.5) | async-done | bytes 131104 | tf_op jit(solution)/shard_map/all_to_all | solution.py:205
  299.7 0.9 fusion.118
  (56 shorter events, 0.4 us)
Async XLA Ops:
  6.5 99.3 %copy-start = (bf16[256,2048]{1,0:T(8,128)(2,1)S(1)}, bf16[256,2048]{1,0:T(8,128)(2,1)}, u32[]{:S(2)}) copy-start(bf16[256,2048]{1,0:T(8,128)(2,1)} %param.39) | copy-start | bytes 3145732
  6.5 84.8 %all-gather.2.cloned.1.call-start = ((), (), s32[]{:S(2)}) async-start(), calls=%async_computation.6 | async-start | bytes 6488064 | tf_op jit(solution)/shard_map/all_gather | solution.py:21
  102.6 3.2 %copy-start.5 = (f32[256]{0:T(256)S(1)}, f32[256]{0:T(256)}, u32[]{:S(2)}) copy-start(f32[256]{0:T(256)} %param.37) | copy-start | bytes 3076
  105.7 1.0 copy-start.1
  105.7 1.0 copy-start.6
  106.8 9.2 %copy-start.3 = (s32[128,2]{0,1:T(2,128)S(1)}, s32[128,2]{0,1:T(2,128)}, u32[]{:S(2)}) copy-start(s32[128,2]{0,1:T(2,128)} %param.41) | copy-start | bytes 3076
  108.1 17.4 %all-to-all-start = ((bf16[16,128,128]{2,1,0:T(8,128)(2,1)}), bf16[16,128,128]{2,1,0:T(8,128)(2,1)S(1)}, u32[]{:S(2)}, u32[]{:S(2)}) async-start(bf16[16,128,128]{2,1,0:T(8,128)(2,1)} %bitcast.270), calls=%async_computation | async-start | bytes 1048576 | tf_op jit(solution)/shard_map/all_to_all | solution.py:32
  127.0 9.8 %all-to-all-start.1 = ((f32[16,1,128]{2,1,0:T(1,128)}), f32[16,1,128]{2,1,0:T(1,128)S(1)}, u32[]{:S(2)}, u32[]{:S(2)}) async-start(f32[16,1,128]{2,1,0:T(1,128)} %broadcast_in_dim.122), calls=%async_computation.1 | async-start | bytes 16384 | tf_op jit(solution)/shard_map/all_to_all | solution.py:38
  239.1 2.4 copy-start.7
  241.5 1.0 copy-start.8
  242.6 1.0 copy-start.2
  273.1 10.8 %copy-start.4 = (f32[128,2]{0,1:T(2,128)S(1)}, f32[128,2]{0,1:T(2,128)}, u32[]{:S(2)}) copy-start(f32[128,2]{0,1:T(2,128)} %param.42) | copy-start | bytes 3076
  274.0 25.7 %all-to-all-start.5 = ((bf16[32,16,128]{2,1,0:T(8,128)(2,1)}), bf16[32,16,128]{2,1,0:T(8,128)(2,1)S(1)}, u32[]{:S(2)}, u32[]{:S(2)}) async-start(bf16[32,16,128]{2,1,0:T(8,128)(2,1)} %reduce_sum.144), calls=%async_computation.5 | async-start | bytes 262144 | tf_op jit(solution)/shard_map/all_to_all | solution.py:205
Sparse Core Ops, SparseCore 0:
  9.5 81.8 all-gather.1
where the time goes:
time: 309 us; the launch traced here: 307 us
  blocking collectives  130 us (42%)
  waiting for transfers between devices  111 us (36%)
  starting transfers between devices  19.8 us (6%)
  local copies, waits for them, and re-layouts  17.3 us (6%)
  between operations  13.7 us (4%)
  matrix products  10.4 us (3%)
  other arithmetic  5.21 us (2%)
    all_gather x1, waiting for transfers between devices, side_by_side(): lax.all_gather(both, axis, axis=dim, tiled=True)  80.3 us
    all_to_all x1, blocking collectives, local(): lax.all_to_all(send_rows, 'sp', split_axis=0, concat_axis=0, tiled=True)  72 us
    all_to_all x1, blocking collectives, sent_to_all(): return lax.all_to_all(copies, axis, split_axis=0, concat_axis=0, tiled=True)  29.6 us
    all_to_all x1, blocking collectives, summed_on_arrival(): lax.all_to_all(pieces, axis, split_axis=0, concat_axis=0, tiled=True)  28.2 us
    all_to_all x1, waiting for transfers between devices, local(): lax.all_to_all(results, 'sp', split_axis=0, concat_axis=0, tiled=True)  15.7 us
    all_to_all x1, starting transfers between devices, local(): lax.all_to_all(results, 'sp', split_axis=0, concat_axis=0, tiled=True)  9.85 us
    all_to_all x1, waiting for transfers between devices, summed_on_arrival(): lax.all_to_all(pieces, axis, split_axis=0, concat_axis=0, tiled=True)  9.52 us
    split x2, local copies, waits for them, and re-layouts, side_by_side(): jnp.split(lax.all_gather(both, axis, axis=dim, tiled=True), ends, axis=al...  6.55 us
  transfers between devices with their start and end apart: 4, of which 4 were waited for; matrix products, arithmetic and copies ran while one was open for 2% of the time, Pallas kernels for 0%

commit v1 on v0

--- a/solution.py
+++ b/solution.py
@@ -7,6 +7,7 @@
 DK_B = 128
 SEG = 64
 TOP = 2
+GROUP = 4
 
 
 EPS = 1e-06
@@ -33,24 +34,19 @@
     return arrived.astype(jnp.float32).sum(axis=0)
 
 
-def sent_to_all(value, axis):
-    copies = jnp.broadcast_to(value, (lax.axis_size(axis), *value.shape))
-    return lax.all_to_all(copies, axis, split_axis=0, concat_axis=0, tiled=True)
-
-
-def over_copies(value, axis):
-    everything = sent_to_all(value, axis)
-    return jnp.sum(everything, axis=0)
-
-
 def in_order(pieces, dim):
     pieces = jnp.moveaxis(pieces, 0, dim)
     dims = pieces.shape
     return pieces.reshape(*dims[:dim], dims[dim] * dims[dim + 1], *dims[dim + 2 :])
 
 
-def gather_directly(value, axis, dim):
-    return in_order(sent_to_all(value, axis), dim)
+def over_lines(value, count, dim):
+    width = count // GROUP
+    blocks = [value]
+    for step in range(1, GROUP):
+        pairs = [(i, (i + step * width) % count) for i in range(count)]
+        blocks.append(lax.ppermute(value, "tp", pairs))
+    return jnp.concatenate(blocks, axis=dim)
 
 
 def attend_local(queries, keys_all, values_all, mixing, head_gain, key_size, offset, block_rows):
@@ -147,6 +143,9 @@
     every_keys_a, every_values_a, every_keys_b, every_values_b = side_by_side(
         (keys_a, values_a, keys_b, values_b), "sp", 0, 2
     )
+    wide_gate = over_lines(expert_gate[0], head_devices, 1)
+    wide_up = over_lines(expert_up[0], head_devices, 1)
+    wide_down = over_lines(expert_down[0], head_devices, 0)
     block_rows = 512
     heads_a = attend_local(
         query_a, every_keys_a, every_values_a, lambda_a, gain_a, DK_A, offset, block_rows
@@ -164,13 +163,7 @@
     col_start = head_index * columns
     summed_cols = summed_on_arrival(partial_branch.astype(jnp.bfloat16), "tp", 1)
     residual_cols = lax.dynamic_slice_in_dim(residual, col_start, columns, 1)
-    stream_cols = (
-        (residual_cols.astype(jnp.float32) + summed_cols).astype(jnp.bfloat16).astype(jnp.float32)
-    )
-    squares = over_copies(jnp.sum(stream_cols * stream_cols, axis=1), "tp")
-    row_scale = lax.rsqrt(squares / model_width + EPS)
-    gain_cols = lax.dynamic_slice_in_dim(norm_gain, col_start, columns, 0)
-    normed_cols = (stream_cols * row_scale[:, None] * gain_cols).astype(jnp.bfloat16)
+    stream_cols = (residual_cols.astype(jnp.float32) + summed_cols).astype(jnp.bfloat16)
     slot_count = 2 * tok_rows * TOP // seq_devices
     assign = routes.reshape(-1)
     onehot = (assign[:, None] == jnp.arange(seq_devices, dtype=jnp.int32)[None, :]).astype(
@@ -186,26 +179,40 @@
     gates = route_weight / jnp.sum(route_weight, axis=1, keepdims=True)
     combine = jnp.sum(placed.astype(jnp.float32) * gates[:, :, None], axis=1)
     send_rows = jnp.einsum(
-        "ts,td->sd", select, normed_cols, preferred_element_type=jnp.float32
+        "ts,td->sd", select, stream_cols, preferred_element_type=jnp.float32
     ).astype(jnp.bfloat16)
     send_rows = send_rows.reshape(seq_devices, slot_count, columns)
-    routed_rows = gather_directly(
-        lax.all_to_all(send_rows, "sp", split_axis=0, concat_axis=0, tiled=True), "tp", 2
-    )
-    sources = routed_rows.shape[0]
-    count = routed_rows.shape[1]
-    flat_rows = routed_rows.reshape(-1, model_width)
-    gate_val = jnp.dot(flat_rows, expert_gate[0], preferred_element_type=jnp.float32)
-    up_val = jnp.dot(flat_rows, expert_up[0], preferred_element_type=jnp.float32)
+    routed = lax.all_to_all(send_rows, "sp", split_axis=0, concat_axis=0, tiled=True)
+    group_rows = seq_devices * slot_count // GROUP
+    grouped = routed.reshape(GROUP, 1, group_rows, columns)
+    copies = jnp.broadcast_to(grouped, (GROUP, head_devices // GROUP, group_rows, columns))
+    arrived = lax.all_to_all(
+        copies.reshape(head_devices, group_rows, columns),
+        "tp",
+        split_axis=0,
+        concat_axis=0,
+        tiled=True,
+    )
+    rows = in_order(arrived, 1).astype(jnp.float32)
+    squares = jnp.sum(rows * rows, axis=1, keepdims=True)
+    normed = (rows * lax.rsqrt(squares / model_width + EPS) * norm_gain).astype(jnp.bfloat16)
+    gate_val = jnp.dot(normed, wide_gate, preferred_element_type=jnp.float32)
+    up_val = jnp.dot(normed, wide_up, preferred_element_type=jnp.float32)
     hidden = (jax.nn.silu(gate_val) * up_val).astype(jnp.bfloat16)
-    down_part = jnp.dot(hidden, expert_down[0], preferred_element_type=jnp.float32).reshape(
-        sources, count, model_width
-    )
-    results = summed_on_arrival(down_part.astype(jnp.bfloat16), "tp", 2).astype(jnp.bfloat16)
+    down_part = jnp.dot(hidden, wide_down, preferred_element_type=jnp.float32)
+    parts = split_up(down_part.astype(jnp.bfloat16), 1, head_devices)
+    parts = lax.all_to_all(parts, "tp", split_axis=0, concat_axis=0, tiled=True)
+    results = (
+        parts.reshape(GROUP, head_devices // GROUP, group_rows, columns)
+        .astype(jnp.float32)
+        .sum(axis=1)
+        .astype(jnp.bfloat16)
+        .reshape(seq_devices, slot_count, columns)
+    )
     returned = lax.all_to_all(results, "sp", split_axis=0, concat_axis=0, tiled=True)
     returned_flat = returned.reshape(seq_devices * slot_count, columns).astype(jnp.float32)
     experts_sum = jnp.dot(combine, returned_flat, precision=lax.Precision.HIGHEST)
-    return (stream_cols + experts_sum).astype(jnp.bfloat16)
+    return (stream_cols.astype(jnp.float32) + experts_sum).astype(jnp.bfloat16)
 
 
 def solution(mesh):

time: 309 us -> 329 us (1.065)
  blocking collectives: 130 us -> 84.5 us
  waiting for transfers between devices: 111 us -> 155 us
  starting transfers between devices: 19.8 us -> 40.3 us
    ppermute x0 -> x9, waiting for transfers between devices: none -> 49.1 us  [over_lines(): blocks.append(lax.ppermute(value, 'tp', pairs))]
    all_to_all x2 -> x1, blocking collectives: 57.8 us -> 13.6 us  [local(): parts = lax.all_to_all(parts, 'tp', split_axis=0, concat_axis=0, tiled=True)]
    ppermute x0 -> x9, starting transfers between devices: none -> 24.7 us  [over_lines(): blocks.append(lax.ppermute(value, 'tp', pairs))]
    all_to_all x1, waiting for transfers between devices: 5.41 us -> 0.01 us  [local(): lax.all_to_all(copies.reshape(head_devices, group_rows, columns), 'tp', s...]
    all_to_all x1, starting transfers between devices: 9.85 us -> 5.51 us  [local(): lax.all_to_all(results, 'sp', split_axis=0, concat_axis=0, tiled=True)]
  transfers between devices with their start and end apart: 4 -> 13, of which waited for: 4 -> 9; matrix products, arithmetic and copies ran while one was open for 2% -> 2% of each run, Pallas kernels for 0% -> 0%
where the time goes in v1:
time: 329 us; the launch traced here: 328 us
  waiting for transfers between devices  155 us (47%)
  blocking collectives  84.5 us (26%)
  starting transfers between devices  40.3 us (12%)
  local copies, waits for them, and re-layouts  14.8 us (4%)
  between operations  13.8 us (4%)
  matrix products  13.6 us (4%)
  other arithmetic  5.51 us (2%)
    all_gather x1, waiting for transfers between devices, side_by_side(): lax.all_gather(both, axis, axis=dim, tiled=True)  79.7 us
    all_to_all x1, blocking collectives, local(): lax.all_to_all(send_rows, 'sp', split_axis=0, concat_axis=0, tiled=True)  70.8 us
    ppermute x9, waiting for transfers between devices, over_lines(): blocks.append(lax.ppermute(value, 'tp', pairs))  49.1 us
    ppermute x9, starting transfers between devices, over_lines(): blocks.append(lax.ppermute(value, 'tp', pairs))  24.7 us
    all_to_all x1, waiting for transfers between devices, local(): lax.all_to_all(results, 'sp', split_axis=0, concat_axis=0, tiled=True)  16 us
    all_to_all x1, blocking collectives, local(): parts = lax.all_to_all(parts, 'tp', split_axis=0, concat_axis=0, tiled=True)  13.6 us
    all_to_all x1, waiting for transfers between devices, summed_on_arrival(): lax.all_to_all(pieces, axis, split_axis=0, concat_axis=0, tiled=True)  9.95 us
  transfers between devices with their start and end apart: 13, of which 9 were waited for; matrix products, arithmetic and copies ran while one was open for 2% of the time, Pallas kernels for 0%

profile of v1, /device:TPU:1, one launch (start us, length us, event | category | flops | bytes accessed | tf_op | source)
XLA Modules:
  0.0 327.6 jit_solution(13453636153118564301)
XLA Ops:
  6.5 1.7 pad_maximum_fusion
  8.2 0.9 fusion.165
  9.3 0.8 copy.90
  10.1 0.1 eq.43
  10.3 0.6 reduce-window.6
  10.9 0.8 fusion.164
  11.7 79.7 %all-gather.2.cloned.1.call-done = bf16[4096,1,768]{2,0,1:T(8,128)(2,1)} async-done(((bf16[128,1,768]{2,0,1:T(8,128)(2,1)}), bf16[4096,1,768]{2,0,1:T(8,128)(2,1)}) %all-gather.2.cloned.1.call-update) | async-done | bytes 6291472 | tf_op jit(solution)/shard_map/all_gather | solution.py:22
  91.4 2.7 fusion.162
  94.1 0.5 copy.88
  94.6 0.9 while.64
  94.7 0.3 fusion.188
  95.1 0.3 fusion.189
  95.5 2.3 while.65
  95.6 0.9 fusion.193
  96.5 1.3 fusion.194
  97.9 3.9 %fusion.163 = (bf16[4096,1,256]{2,0,1:T(8,128)(2,1)S(1)}, bf16[4096,1,256]{2,0,1:T(8,128)(2,1)}) fusion(bf16[4096,1,768]{2,0,1:T(8,128)(2,1)} %all-gather.2.cloned.1.call-done), kind=kLoop, calls=%fused_computation.243 | loop fusion | bytes 8388608 | tf_op jit(solution)/shard_map/split | solution.py:22
  101.8 0.8 while.66
  101.8 0.2 fusion.195
  102.2 0.2 fusion.196
  102.6 3.1 while.67
  102.6 0.9 fusion.200
  103.6 2.1 fusion.201
  105.8 0.4 fusion.142
  106.2 0.5 copy-done.1
  106.8 0.4 fusion.130
  107.2 0.9 copy.108
  108.1 6.5 %all-to-all-start = ((bf16[16,128,128]{2,1,0:T(8,128)(2,1)}), bf16[16,128,128]{2,1,0:T(8,128)(2,1)S(1)}, u32[]{:S(2)}, u32[]{:S(2)}) async-start(bf16[16,128,128]{2,1,0:T(8,128)(2,1)} %bitcast.264), calls=%async_computation | async-start | bytes 1048576 | tf_op jit(solution)/shard_map/all_to_all | solution.py:33
  114.7 0.2 slice_reduce_fusion
  114.8 0.1 eq.39
  115.1 0.1 reduce_sum.129
  115.4 0.1 fusion.135
  115.5 9.9 %all-to-all-done = bf16[16,128,128]{2,1,0:T(8,128)(2,1)S(1)} async-done(((bf16[16,128,128]{2,1,0:T(8,128)(2,1)}), bf16[16,128,128]{2,1,0:T(8,128)(2,1)S(1)}, u32[]{:S(2)}, u32[]{:S(2)}) %all-to-all-start) | async-done | bytes 524320 | tf_op jit(solution)/shard_map/all_to_all | solution.py:33
  125.5 0.8 add_convert_fusion
  126.3 0.2 convolution_convert_fusion.1
  126.5 70.8 %all_to_all.25 = bf16[32,16,128]{2,1,0:T(8,128)(2,1)S(1)} all-to-all(bf16[32,16,128]{2,1,0:T(8,128)(2,1)S(1)} %bitcast.355), channel_id=1, replica_groups=mesh['sp'=32,'tp'=16] {'sp'}, dimensions={0} | all-to-all | bytes 262144 | tf_op jit(solution)/shard_map/all_to_all | solution.py:185
  197.5 0.9 broadcast_in_dim.124
  198.4 3.6 %all-to-all-start.2 = ((bf16[16,128,128]{1,2,0:T(8,128)(2,1)}), bf16[16,128,128]{1,2,0:T(8,128)(2,1)S(1)}, u32[]{:S(2)}, u32[]{:S(2)}) async-start(bf16[16,128,128]{1,2,0:T(8,128)(2,1)} %bitcast.8), calls=%async_computation.2 | async-start | bytes 1048576 | tf_op jit(solution)/shard_map/all_to_all | solution.py:189
  202.0 3.2 collective-permute-start
  205.2 4.4 %collective-permute-start.1 = (bf16[2048,128]{1,0:T(8,128)(2,1)S(1)}, bf16[2048,128]{1,0:T(8,128)(2,1)}, u32[]{:S(2)}, u32[]{:S(2)}) collective-permute-start(bf16[2048,128]{1,0:T(8,128)(2,1)S(1)} %bitcast.370), channel_id=1, source_target_pairs={{0,8},{1,9},{2,10},{3,11},{4,12},{5,13},{6,14},{7,15},{8,0},{9,1},... | collective-permute-start | bytes 1572872 | tf_op jit(solution)/shard_map/ppermute | solution.py:48
  209.6 3.1 collective-permute-start.2
  212.6 2.2 collective-permute-start.3
  214.9 2.8 collective-permute-start.4
  217.7 0.3 multiply_reduce_fusion
  218.0 5.6 %collective-permute-done = bf16[2048,128]{1,0:T(8,128)(2,1)} collective-permute-done((bf16[2048,128]{1,0:T(8,128)(2,1)S(1)}, bf16[2048,128]{1,0:T(8,128)(2,1)}, u32[]{:S(2)}, u32[]{:S(2)}) %collective-permute-start) | collective-permute-done | bytes 524320 | tf_op jit(solution)/shard_map/ppermute | solution.py:48
  223.5 2.5 collective-permute-start.5
  226.0 9.1 %collective-permute-done.1 = bf16[2048,128]{1,0:T(8,128)(2,1)} collective-permute-done((bf16[2048,128]{1,0:T(8,128)(2,1)S(1)}, bf16[2048,128]{1,0:T(8,128)(2,1)}, u32[]{:S(2)}, u32[]{:S(2)}) %collective-permute-start.1) | collective-permute-done | bytes 524320 | tf_op jit(solution)/shard_map/ppermute | solution.py:48
  235.1 1.9 collective-permute-start.6
  237.1 2.1 collective-permute-start.7
  239.2 6.8 %collective-permute-done.3 = bf16[2048,128]{1,0:T(8,128)(2,1)S(1)} collective-permute-done((bf16[2048,128]{1,0:T(8,128)(2,1)}, bf16[2048,128]{1,0:T(8,128)(2,1)S(1)}, u32[]{:S(2)}, u32[]{:S(2)}) %collective-permute-start.3) | collective-permute-done | bytes 524320 | tf_op jit(solution)/shard_map/ppermute | solution.py:48
  245.9 0.8 copy-done.9
  246.7 2.6 collective-permute-start.8
  249.4 0.3 fusion.133
  249.7 2.6 fusion.104
  252.3 5.3 %collective-permute-done.4 = bf16[2048,128]{1,0:T(8,128)(2,1)} collective-permute-done((bf16[2048,128]{1,0:T(8,128)(2,1)}, bf16[2048,128]{1,0:T(8,128)(2,1)}, u32[]{:S(2)}, u32[]{:S(2)}) %collective-permute-start.4) | collective-permute-done | bytes 524320 | tf_op jit(solution)/shard_map/ppermute | solution.py:48
  257.7 10.7 %collective-permute-done.6 = bf16[128,2048]{1,0:T(8,128)(2,1)S(1)} collective-permute-done((bf16[128,2048]{1,0:T(8,128)(2,1)S(1)}, bf16[128,2048]{1,0:T(8,128)(2,1)S(1)}, u32[]{:S(2)}, u32[]{:S(2)}) %collective-permute-start.6) | collective-permute-done | bytes 524320 | tf_op jit(solution)/shard_map/ppermute | solution.py:48
  268.4 11.6 %collective-permute-done.7 = bf16[128,2048]{1,0:T(8,128)(2,1)S(1)} collective-permute-done((bf16[128,2048]{1,0:T(8,128)(2,1)S(1)}, bf16[128,2048]{1,0:T(8,128)(2,1)S(1)}, u32[]{:S(2)}, u32[]{:S(2)}) %collective-permute-start.7) | collective-permute-done | bytes 524320 | tf_op jit(solution)/shard_map/ppermute | solution.py:48
  280.0 0.8 copy-done.13
  280.8 2.8 fusion.127
  283.8 13.6 %all_to_all.26 = bf16[16,128,128]{2,1,0:T(8,128)(2,1)S(1)} all-to-all(bf16[16,128,128]{2,1,0:T(8,128)(2,1)S(1)} %bitcast.353), channel_id=1, replica_groups=mesh['sp'=32,'tp'=16] {'tp'}, dimensions={0} | all-to-all | bytes 1048576 | tf_op jit(solution)/shard_map/all_to_all | solution.py:204
  297.4 0.7 bitcast_reduce_fusion
  298.2 5.5 %all-to-all-start.4 = ((bf16[32,16,128]{2,1,0:T(8,128)(2,1)}), bf16[32,16,128]{2,1,0:T(8,128)(2,1)S(1)}, u32[]{:S(2)}, u32[]{:S(2)}) async-start(bf16[32,16,128]{2,1,0:T(8,128)(2,1)} %bitcast.16), calls=%async_computation.4 | async-start | bytes 262144 | tf_op jit(solution)/shard_map/all_to_all | solution.py:212
  303.7 0.1 select_reduce_fusion
  303.9 16.0 %all-to-all-done.4 = bf16[32,16,128]{2,1,0:T(8,128)(2,1)S(1)} async-done(((bf16[32,16,128]{2,1,0:T(8,128)(2,1)}), bf16[32,16,128]{2,1,0:T(8,128)(2,1)S(1)}, u32[]{:S(2)}, u32[]{:S(2)}) %all-to-all-start.4) | async-done | bytes 131104 | tf_op jit(solution)/shard_map/all_to_all | solution.py:212
  319.9 0.9 fusion.131
  (81 shorter events, 1.5 us)
Async XLA Ops:
  6.5 99.3 %copy-start = (bf16[256,2048]{1,0:T(8,128)(2,1)S(1)}, bf16[256,2048]{1,0:T(8,128)(2,1)}, u32[]{:S(2)}) copy-start(bf16[256,2048]{1,0:T(8,128)(2,1)} %param.39) | copy-start | bytes 3145732
  6.5 84.8 %all-gather.2.cloned.1.call-start = ((), (), s32[]{:S(2)}) async-start(), calls=%async_computation.5 | async-start | bytes 6488064 | tf_op jit(solution)/shard_map/all_gather | solution.py:22
  102.6 3.2 copy-start.5
  105.7 1.0 copy-start.1
  105.7 1.0 copy-start.6
  106.8 8.6 %copy-start.3 = (s32[128,2]{0,1:T(2,128)S(1)}, s32[128,2]{0,1:T(2,128)}, u32[]{:S(2)}) copy-start(s32[128,2]{0,1:T(2,128)} %param.41) | copy-start | bytes 3076
  108.1 17.3 %all-to-all-start = ((bf16[16,128,128]{2,1,0:T(8,128)(2,1)}), bf16[16,128,128]{2,1,0:T(8,128)(2,1)S(1)}, u32[]{:S(2)}, u32[]{:S(2)}) async-start(bf16[16,128,128]{2,1,0:T(8,128)(2,1)} %bitcast.264), calls=%async_computation | async-start | bytes 1048576 | tf_op jit(solution)/shard_map/all_to_all | solution.py:33
  114.6 87.4 %copy-start.7 = (bf16[1,2048,128]{2,1,0:T(8,128)(2,1)S(1)}, bf16[1,2048,128]{2,1,0:T(8,128)(2,1)}, u32[]{:S(2)}) copy-start(bf16[1,2048,128]{2,1,0:T(8,128)(2,1)} %param.43) | copy-start | bytes 1572868
  114.6 120.5 %copy-start.8 = (bf16[1,128,2048]{2,1,0:T(8,128)(2,1)S(1)}, bf16[1,128,2048]{2,1,0:T(8,128)(2,1)}, u32[]{:S(2)}) copy-start(bf16[1,128,2048]{2,1,0:T(8,128)(2,1)} %param.45) | copy-start | bytes 1572868
  114.7 134.7 %copy-start.2 = (f32[2048]{0:T(1024)S(1)}, f32[2048]{0:T(1024)}, u32[]{:S(2)}) copy-start(f32[2048]{0:T(1024)} %param.40) | copy-start | bytes 24580
  198.4 19.2 %all-to-all-start.2 = ((bf16[16,128,128]{1,2,0:T(8,128)(2,1)}), bf16[16,128,128]{1,2,0:T(8,128)(2,1)S(1)}, u32[]{:S(2)}, u32[]{:S(2)}) async-start(bf16[16,128,128]{1,2,0:T(8,128)(2,1)} %bitcast.8), calls=%async_computation.2 | async-start | bytes 1048576 | tf_op jit(solution)/shard_map/all_to_all | solution.py:189
  202.0 21.5 %collective-permute-start = (bf16[2048,128]{1,0:T(8,128)(2,1)S(1)}, bf16[2048,128]{1,0:T(8,128)(2,1)}, u32[]{:S(2)}, u32[]{:S(2)}) collective-permute-start(bf16[2048,128]{1,0:T(8,128)(2,1)S(1)} %bitcast.369), channel_id=1, source_target_pairs={{0,4},{1,5},{2,6},{3,7},{4,8},{5,9},{6,10},{7,11},{8,12},{9,13},{1... | collective-permute-start | bytes 1572872 | tf_op jit(solution)/shard_map/ppermute | solution.py:48
  205.2 29.9 %collective-permute-start.1 = (bf16[2048,128]{1,0:T(8,128)(2,1)S(1)}, bf16[2048,128]{1,0:T(8,128)(2,1)}, u32[]{:S(2)}, u32[]{:S(2)}) collective-permute-start(bf16[2048,128]{1,0:T(8,128)(2,1)S(1)} %bitcast.370), channel_id=1, source_target_pairs={{0,8},{1,9},{2,10},{3,11},{4,12},{5,13},{6,14},{7,15},{8,0},{9,1},... | collective-permute-start | bytes 1572872 | tf_op jit(solution)/shard_map/ppermute | solution.py:48
  209.6 27.5 %collective-permute-start.2 = (bf16[2048,128]{1,0:T(8,128)(2,1)S(1)}, bf16[2048,128]{1,0:T(8,128)(2,1)}, u32[]{:S(2)}, u32[]{:S(2)}) collective-permute-start(bf16[2048,128]{1,0:T(8,128)(2,1)S(1)} %bitcast.371), channel_id=1, source_target_pairs={{0,12},{1,13},{2,14},{3,15},{4,0},{5,1},{6,2},{7,3},{8,4},{9,5},{1... | collective-permute-start | bytes 1572872 | tf_op jit(solution)/shard_map/ppermute | solution.py:48
  212.6 33.3 %collective-permute-start.3 = (bf16[2048,128]{1,0:T(8,128)(2,1)}, bf16[2048,128]{1,0:T(8,128)(2,1)S(1)}, u32[]{:S(2)}, u32[]{:S(2)}) collective-permute-start(bf16[2048,128]{1,0:T(8,128)(2,1)} %bitcast.12), channel_id=1, source_target_pairs={{0,4},{1,5},{2,6},{3,7},{4,8},{5,9},{6,10},{7,11},{8,12},{9,13},{1... | collective-permute-start | bytes 1572872 | tf_op jit(solution)/shard_map/ppermute | solution.py:48
  214.9 42.8 %collective-permute-start.4 = (bf16[2048,128]{1,0:T(8,128)(2,1)}, bf16[2048,128]{1,0:T(8,128)(2,1)}, u32[]{:S(2)}, u32[]{:S(2)}) collective-permute-start(bf16[2048,128]{1,0:T(8,128)(2,1)} %bitcast.12), channel_id=1, source_target_pairs={{0,8},{1,9},{2,10},{3,11},{4,12},{5,13},{6,14},{7,15},{8,0},{9,1},... | collective-permute-start | bytes 1572872 | tf_op jit(solution)/shard_map/ppermute | solution.py:48
  223.5 34.1 %collective-permute-start.5 = (bf16[2048,128]{1,0:T(8,128)(2,1)}, bf16[2048,128]{1,0:T(8,128)(2,1)S(1)}, u32[]{:S(2)}, u32[]{:S(2)}) collective-permute-start(bf16[2048,128]{1,0:T(8,128)(2,1)} %bitcast.12), channel_id=1, source_target_pairs={{0,12},{1,13},{2,14},{3,15},{4,0},{5,1},{6,2},{7,3},{8,4},{9,5},{1... | collective-permute-start | bytes 1572872 | tf_op jit(solution)/shard_map/ppermute | solution.py:48
  235.1 33.2 %collective-permute-start.6 = (bf16[128,2048]{1,0:T(8,128)(2,1)S(1)}, bf16[128,2048]{1,0:T(8,128)(2,1)S(1)}, u32[]{:S(2)}, u32[]{:S(2)}) collective-permute-start(bf16[128,2048]{1,0:T(8,128)(2,1)S(1)} %bitcast.373), channel_id=1, source_target_pairs={{0,4},{1,5},{2,6},{3,7},{4,8},{5,9},{6,10},{7,11},{8,12},{9,13},{1... | collective-permute-start | bytes 1572872 | tf_op jit(solution)/shard_map/ppermute | solution.py:48
  237.1 42.9 %collective-permute-start.7 = (bf16[128,2048]{1,0:T(8,128)(2,1)S(1)}, bf16[128,2048]{1,0:T(8,128)(2,1)S(1)}, u32[]{:S(2)}, u32[]{:S(2)}) collective-permute-start(bf16[128,2048]{1,0:T(8,128)(2,1)S(1)} %bitcast.374), channel_id=1, source_target_pairs={{0,8},{1,9},{2,10},{3,11},{4,12},{5,13},{6,14},{7,15},{8,0},{9,1},... | collective-permute-start | bytes 1572872 | tf_op jit(solution)/shard_map/ppermute | solution.py:48
  245.9 0.8 copy-start.9
  246.7 34.1 %collective-permute-start.8 = (bf16[128,2048]{1,0:T(8,128)(2,1)S(1)}, bf16[128,2048]{1,0:T(8,128)(2,1)}, u32[]{:S(2)}, u32[]{:S(2)}) collective-permute-start(bf16[128,2048]{1,0:T(8,128)(2,1)S(1)} %bitcast.375), channel_id=1, source_target_pairs={{0,12},{1,13},{2,14},{3,15},{4,0},{5,1},{6,2},{7,3},{8,4},{9,5},{1... | collective-permute-start | bytes 1572872 | tf_op jit(solution)/shard_map/ppermute | solution.py:48
  249.7 31.1 %copy-start.10 = (bf16[2048,128]{1,0:T(8,128)(2,1)S(1)}, bf16[2048,128]{1,0:T(8,128)(2,1)}, u32[]{:S(2)}) copy-start(bf16[2048,128]{1,0:T(8,128)(2,1)} %copy-done.9) | copy-start | bytes 1572868
  257.7 22.4 %copy-start.11 = (bf16[2048,128]{1,0:T(8,128)(2,1)}, bf16[2048,128]{1,0:T(8,128)(2,1)S(1)}, u32[]{:S(2)}) copy-start(bf16[2048,128]{1,0:T(8,128)(2,1)S(1)} %collective-permute-done.5) | copy-start | bytes 1572868
  268.4 11.6 %copy-start.12 = (bf16[128,2048]{1,0:T(8,128)(2,1)}, bf16[128,2048]{1,0:T(8,128)(2,1)S(1)}, u32[]{:S(2)}) copy-start(bf16[128,2048]{1,0:T(8,128)(2,1)S(1)} %collective-permute-done.6) | copy-start | bytes 1572868
  280.0 0.8 copy-start.13
  283.7 20.0 %copy-start.4 = (f32[128,2]{0,1:T(2,128)S(1)}, f32[128,2]{0,1:T(2,128)}, u32[]{:S(2)}) copy-start(f32[128,2]{0,1:T(2,128)} %param.42) | copy-start | bytes 3076
  298.2 21.7 %all-to-all-start.4 = ((bf16[32,16,128]{2,1,0:T(8,128)(2,1)}), bf16[32,16,128]{2,1,0:T(8,128)(2,1)S(1)}, u32[]{:S(2)}, u32[]{:S(2)}) async-start(bf16[32,16,128]{2,1,0:T(8,128)(2,1)} %bitcast.16), calls=%async_computation.4 | async-start | bytes 262144 | tf_op jit(solution)/shard_map/all_to_all | solution.py:212
Sparse Core Ops, SparseCore 0:
  9.5 81.8 all-gather.1
